TPU v7x, 32 devices: a whole 2x2x4 slice. The times are simulated.
32 devices in a mesh: ep: 4 (over y, x), tp: 8 (over z, core).
Axes of the slice: x: 2, y: 2, z: 4, core: 2. Of those that a mesh axis runs over, the one named last changes fastest.
Arguments:
- query_heads_rows: bfloat16 [2048, 2048], P('ep', 'tp'), may hold values from -9 to 9
- key_heads_rows: bfloat16 [2048, 2048], P('ep', 'tp'), may hold values from -9 to 9
- value_heads_rows: bfloat16 [2048, 2048], P('ep', 'tp'), may hold values from -6 to 6
- write_strength_logit: bfloat16 [16, 2048], P('tp', 'ep'), may hold values from -3.5 to -1
- decay_preactivation: bfloat16 [16, 2048], P('tp', 'ep'), may hold values from -5 to 5
- head_decay_logarithm: float32 [16], P('tp'), may hold values from -20 to -3
- extra_log_decay: float32 [16, 2048], P('tp', 'ep'), may hold values from -0.7 to 0
- output_weight: bfloat16 [2048, 2048], P('tp'), may hold values from -2 to 2
- second_batch_tokens: bfloat16 [4096, 2048], P(('ep', 'tp')), may hold values from -6 to 6
- expert_norm_scale: float32 [2048], replicated, may hold values from 0.1 to 1.9
- expert_choice_index: int32 [4096, 2], P(('ep', 'tp')), may hold values from 0 to 15, as said below
- group_router_weight: float32 [4096], P(('ep', 'tp')), may hold values from 0.25 to 1
- expert_logit_difference: float32 [4096], P(('ep', 'tp')), may hold values from -8 to 8
- expert_gate_weight: bfloat16 [16, 1024, 2048], P('ep', 'tp'), may hold values from -0.125 to 0.125
- expert_up_weight: bfloat16 [16, 1024, 2048], P('ep', 'tp'), may hold values from -0.125 to 0.125
- expert_down_weight: bfloat16 [16, 1024, 2048], P('ep', 'tp'), may hold values from -0.375 to 0.375
Outputs:
- mixer_output_first: bfloat16 [2048, 2048], P(('ep', 'tp'))
- expert_out: bfloat16 [4096, 2048], P(('ep', 'tp'))
Inputs may be any that keep to these rules, and one draw needn't show every extreme that they name: `expert_choice_index`: each row names two different experts of one group, the experts a * 4 to a * 4 + 3 for some a. In the rows of one device (aligned blocks of 128 rows) no expert is named more than 32 times, and in every device's rows some expert is named exactly 32 times.
All inputs are finite; a program needn't handle non-finite values.
Results may differ from a plain program's by a relative error of at most 0.018.
Values may be sent and summed in bfloat16 or wider, within the bound.
A program may use at most 128 MiB of HBM per device.

v0:
```python
import jax
import jax.numpy as jnp
from jax import lax
from jax.sharding import PartitionSpec as P

DK = 128
DV = 128
BLOCK = 64
CAP = 32
EXPERTS = 16
TOPK = 2
precise_setting = lax.Precision.HIGHEST
norm_eps = 1e-06


def prefix(value, axis, join, neutral):
    count, mine = (lax.axis_size(axis), lax.axis_index(axis))
    pieces = jax.tree.map(lambda part: lax.all_gather(part, axis), value)
    subtotal = jax.tree.map(
        lambda part, zero: jnp.full_like(part, 0) + jnp.asarray(zero, part.dtype), value, neutral
    )

    def step(position, subtotal):
        longer = join(subtotal, jax.tree.map(lambda part: part[position], pieces))
        return jax.tree.map(lambda new, old: jnp.where(position < mine, new, old), longer, subtotal)

    return lax.fori_loop(0, count - 1, step, subtotal)


def unit_rows(matrix):
    return matrix * lax.rsqrt(jnp.sum(matrix * matrix, axis=-1, keepdims=True) + norm_eps)


def block_terms(query_block, key_block, value_block, decay_logarithm, strength):
    span_len = query_block.shape[2]
    dim_value = value_block.shape[-1]
    cumulative = jnp.cumsum(decay_logarithm, axis=-1)
    within = jnp.tril(jnp.ones((span_len, span_len), bool))
    strict = jnp.tril(jnp.ones((span_len, span_len), bool), -1)
    spread = cumulative[..., :, None] - cumulative[..., None, :]
    decayed = jnp.where(within, jnp.exp(jnp.where(within, spread, 0.0)), 0.0)
    weighted = key_block * strength[..., None]
    lower_part = jnp.where(
        strict,
        jnp.einsum("hnid,hnjd->hnij", weighted, key_block, precision=precise_setting) * decayed,
        0.0,
    )
    system = lower_part + jnp.eye(span_len, dtype=jnp.float32)
    rhs_cols = jnp.concatenate(
        [value_block * strength[..., None], weighted * jnp.exp(cumulative)[..., None]], axis=-1
    )
    solved = jax.scipy.linalg.solve_triangular(system, rhs_cols, lower=True, unit_diagonal=True)
    updated_values = solved[..., :dim_value]
    delta_corrections = solved[..., dim_value:]
    scores = jnp.where(
        within,
        jnp.einsum("hnid,hnjd->hnij", query_block, key_block, precision=precise_setting) * decayed,
        0.0,
    )
    decayed_queries = query_block * jnp.exp(cumulative)[..., None]
    decayed_keys = key_block * jnp.exp(cumulative[..., -1:] - cumulative)[..., None]
    block_retention = jnp.exp(cumulative[..., -1])
    return (
        decayed_queries,
        decayed_keys,
        updated_values,
        delta_corrections,
        scores,
        block_retention,
    )


def carry_step(recurrent_state, inputs):
    decayed_queries, decayed_keys, updated_values, delta_corrections, scores, block_retention = (
        inputs
    )
    value_updates = updated_values - jnp.einsum(
        "jdb,jbu->jdu", delta_corrections, recurrent_state, precision=precise_setting
    )
    final_output = jnp.einsum(
        "jdb,jbu->jdu", decayed_queries, recurrent_state, precision=precise_setting
    )
    final_output = final_output + jnp.einsum(
        "hcj,hjv->hcv", scores, value_updates, precision=precise_setting
    )
    recurrent_state = recurrent_state * block_retention[:, None, None] + jnp.einsum(
        "rpq,rpd->rqd", decayed_keys, value_updates, precision=precise_setting
    )
    return (recurrent_state, final_output)


def compose(earlier, latter):
    joined_map = jnp.einsum("hij,hjk->hik", latter[0], earlier[0], precision=precise_setting)
    joined_state = (
        jnp.einsum("hij,hjv->hiv", latter[0], earlier[1], precision=precise_setting) + latter[1]
    )
    return (joined_map, joined_state)


def shards(
    query_heads_rows,
    key_heads_rows,
    value_heads_rows,
    write_strength_logit,
    decay_preactivation,
    head_decay_logarithm,
    extra_log_decay,
    output_weight,
    second_batch_tokens,
    expert_norm_scale,
    expert_choice_index,
    group_router_weight,
    expert_logit_difference,
    expert_gate_weight,
    expert_up_weight,
    expert_down_weight,
):
    length = query_heads_rows.shape[0]
    local_heads = head_decay_logarithm.shape[0]
    blocks = length // BLOCK
    width_model = output_weight.shape[1]

    def heads_first(matrix):
        spread_out = matrix.astype(jnp.float32).reshape(length, local_heads, -1).transpose(1, 0, 2)
        return spread_out.reshape(local_heads, blocks, BLOCK, -1)

    query_block = unit_rows(heads_first(query_heads_rows)) * DK ** (-0.5)
    key_block = unit_rows(heads_first(key_heads_rows))
    value_block = heads_first(value_heads_rows)
    strength = jax.nn.sigmoid(write_strength_logit.astype(jnp.float32)).reshape(
        local_heads, blocks, BLOCK
    )
    decay_logarithm = (
        -jnp.exp(head_decay_logarithm)[:, None]
        * jax.nn.softplus(decay_preactivation.astype(jnp.float32))
        + extra_log_decay
    )
    decay_logarithm = decay_logarithm.reshape(local_heads, blocks, BLOCK)
    decayed_queries, decayed_keys, updated_values, delta_corrections, scores, block_retention = (
        block_terms(query_block, key_block, value_block, decay_logarithm, strength)
    )
    fresh_wide = jnp.concatenate(
        [updated_values, jnp.zeros(updated_values.shape[:-1] + (DK,), jnp.float32)], axis=-1
    )
    inputs = tuple(
        (
            jnp.moveaxis(term, 1, 0)
            for term in (
                decayed_queries,
                decayed_keys,
                fresh_wide,
                delta_corrections,
                scores,
                block_retention,
            )
        )
    )
    identity_map = jnp.broadcast_to(jnp.eye(DK, dtype=jnp.float32), (local_heads, DK, DK))
    start_memory = jnp.concatenate(
        [jnp.zeros((local_heads, DK, DV), jnp.float32), identity_map], axis=-1
    )
    end_memory, outputs = lax.scan(carry_step, start_memory, inputs)
    local_output = outputs[..., :DV]
    projection_matrix = outputs[..., DV:]
    carried_end = end_memory[..., :DV]
    transfer = end_memory[..., DV:]
    _, incoming_rows = prefix(
        (transfer, carried_end), "ep", compose, (identity_map, jnp.zeros_like(carried_end))
    )
    attention_result = local_output + jnp.einsum(
        "xtyg,tgd->xtyd", projection_matrix, incoming_rows, precision=precise_setting
    )
    attn_rows = (
        attention_result.transpose(0, 2, 1, 3)
        .reshape(length, local_heads * DV)
        .astype(jnp.bfloat16)
    )
    summed = lax.psum_scatter(
        jnp.dot(attn_rows, output_weight, preferred_element_type=jnp.float32).astype(jnp.bfloat16),
        "tp",
        scatter_dimension=0,
        tiled=True,
    )
    widened = second_batch_tokens.astype(jnp.float32)
    normed = (
        widened
        * lax.rsqrt(jnp.mean(widened * widened, axis=-1, keepdims=True) + norm_eps)
        * expert_norm_scale
    ).astype(jnp.bfloat16)
    own_tokens = second_batch_tokens.shape[0]
    ep_count = lax.axis_size("ep")
    local_experts = EXPERTS // ep_count
    flat_ids = expert_choice_index.reshape(-1)
    one_hot = (flat_ids[:, None] == jnp.arange(EXPERTS, dtype=jnp.int32)[None, :]).astype(jnp.int32)
    slot_rank = jnp.sum((jnp.cumsum(one_hot, axis=0) - one_hot) * one_hot, axis=1)
    slot_index = flat_ids * CAP + slot_rank
    copy_token = jnp.arange(flat_ids.shape[0], dtype=jnp.int32) // TOPK
    slot_token = jnp.full((EXPERTS * CAP,), own_tokens, jnp.int32).at[slot_index].set(copy_token)
    outgoing = jnp.take(normed, slot_token, axis=0, mode="fill", fill_value=0).reshape(
        ep_count, local_experts, CAP, width_model
    )
    arrived = lax.all_to_all(outgoing, "ep", split_axis=0, concat_axis=0, tiled=True)
    gate_piece = lax.all_gather(expert_gate_weight, "tp", axis=1, tiled=True)
    up_piece = lax.all_gather(expert_up_weight, "tp", axis=1, tiled=True)
    down_piece = lax.all_gather(expert_down_weight, "tp", axis=1, tiled=True)
    gating = jnp.einsum("secd,efd->secf", arrived, gate_piece, preferred_element_type=jnp.float32)
    upward = jnp.einsum("secd,efd->secf", arrived, up_piece, preferred_element_type=jnp.float32)
    hidden = (jax.nn.silu(gating) * upward).astype(jnp.bfloat16)
    produced = jnp.einsum("secf,efd->secd", hidden, down_piece, preferred_element_type=jnp.float32)
    returned = lax.all_to_all(
        produced.astype(jnp.bfloat16), "ep", split_axis=0, concat_axis=0, tiled=True
    )
    flat_results = returned.reshape(EXPERTS * CAP, width_model)
    picked = (
        jnp.take(flat_results, slot_index, axis=0)
        .reshape(own_tokens, TOPK, width_model)
        .astype(jnp.float32)
    )
    leading = jax.nn.sigmoid(expert_logit_difference)
    mixing = group_router_weight[:, None] * jnp.stack([leading, 1.0 - leading], axis=-1)
    expert_out = jnp.sum(mixing[..., None] * picked, axis=1).astype(jnp.bfloat16)
    return (summed, expert_out)


def solution(mesh):
    in_specs = (
        P("ep", "tp"),
        P("ep", "tp"),
        P("ep", "tp"),
        P("tp", "ep"),
        P("tp", "ep"),
        P("tp"),
        P("tp", "ep"),
        P("tp", None),
        P(("ep", "tp"), None),
        P(),
        P(("ep", "tp"), None),
        P(("ep", "tp")),
        P(("ep", "tp")),
        P("ep", "tp", None),
        P("ep", "tp", None),
        P("ep", "tp", None),
    )
    out_specs = (P(("ep", "tp"), None), P(("ep", "tp"), None))
    return jax.shard_map(shards, mesh=mesh, in_specs=in_specs, out_specs=out_specs, check_vma=False)
```

profile of v0, /device:TPU:0, one launch (start us, length us, event | category | flops | bytes accessed | tf_op | source)
XLA Modules:
  0.0 520.2 jit_solution(1640668718798541853)
XLA Ops:
  11.6 1.4 scatter_custom_fusion
  13.5 3.3 gather_fusion
  16.9 3.1 broadcast_select_fusion
  20.0 5.6 %all-to-all-start = ((bf16[4,4,32,2048]{3,2,1,0:T(8,128)(2,1)}), bf16[4,4,32,2048]{3,2,1,0:T(8,128)(2,1)S(1)}, u32[]{:S(2)}, u32[]{:S(2)}) async-start(bf16[4,4,32,2048]{3,2,1,0:T(8,128)(2,1)} %broadcast_select_fusion), calls=%async_computation.1 | async-start | bytes 4194304 | tf_op jit(solution)/shard_map/all_to_all | solution.py:202
  29.5 3.0 fusion.52
  32.4 80.0 %custom-call.4 = f32[2,8,1,64,64]{3,4,2,1,0:T(8,128)} custom-call(f32[2,8,1,64,64]{4,3,2,1,0:T(8,128)} %fusion.52), custom_call_target="InvertDiagBlocksLowerTriangular" | custom-call | tf_op jit(solution)/shard_map/jit(_solve_triangular)/vmap(vmap())/triangular_solve | solution.py:52
  114.4 2.0 copy.100
  119.9 2.5 multiply_multiply_fusion
  125.6 2.0 fusion.50
  128.6 48.9 %while.26 = (s32[]{:T(128)}, f32[2,128,256]{2,1,0:T(8,128)S(1)}, f32[8,2,64,256]{3,2,0,1:T(8,128)}, f32[8,2]{1,0:T(8,128)}, f32[8,2,64,128]{3,2,0,1:T(8,128)}, /...) while((s32[]{:T(128)}, f32[2,128,256]{2,1,0:T(8,128)S(1)}, ...), condition=%wide.region_4.5_spmd, body=%wide.region_3.4_spmd.sunk | while | flops 176357376 | bytes 2231425 | solution.py:162
  128.6 1.2 convolution_subtract_fusion.2
  131.0 1.8 fusion.127
  133.5 1.3 convolution_add_fusion.4
  137.1 1.8 fusion.127
  139.6 1.3 convolution_add_fusion.4
  143.2 1.8 fusion.127
  145.7 1.3 convolution_add_fusion.4
  149.3 1.8 fusion.127
  151.8 1.3 convolution_add_fusion.4
  155.4 1.8 fusion.127
  157.9 1.3 convolution_add_fusion.4
  161.5 1.8 fusion.127
  164.0 1.3 convolution_add_fusion.4
  165.2 1.2 convolution_subtract_fusion.2
  167.6 1.8 fusion.127
  170.1 1.3 convolution_add_fusion.4
  171.4 1.3 convolution_subtract_fusion.2
  173.8 1.8 fusion.127
  176.3 1.3 convolution_add_fusion.4
  177.6 11.2 %all-gather = f32[8,128,128]{2,1,0:T(8,128)} all-gather(f32[2,128,128]{2,1,0:T(8,128)S(1)} %get-tuple-element.243), channel_id=2, replica_groups=mesh['ep'=4,'tp'=8] {'ep'}, dimensions={0}, use_global_device_ids=true | all-gather | bytes 655360 | tf_op jit(solution)/shard_map/all_gather | solution.py:18
  188.8 11.2 %all-gather.1 = f32[8,128,128]{2,1,0:T(8,128)} all-gather(f32[2,128,128]{2,1,0:T(8,128)S(1)} %get-tuple-element.242), channel_id=3, replica_groups=mesh['ep'=4,'tp'=8] {'ep'}, dimensions={0}, use_global_device_ids=true | all-gather | bytes 655360 | tf_op jit(solution)/shard_map/all_gather | solution.py:18
  200.1 4.0 while.27
  200.1 1.2 fusion.130
  201.4 1.2 fusion.130
  202.7 1.2 fusion.130
  204.1 1.8 fusion.55
  206.2 2.1 convolution_convert_fusion
  208.4 12.9 %fusion.26 = f32[4,4,32,1024]{3,2,1,0:T(8,128)} fusion(bf16[4,1024,2048]{2,1,0:T(8,128)(2,1)} %all-gather.8.cloned.1.call-done, bf16[4,4,32,2048]{3,2,1,0:T(8,128)(2,1)S(1)} %all-to-all-done), kind=kOutput, calls=%fused_computation.34 | convolution fusion | flops 2147483648 | bytes 20971520 | tf_op jit(solution)/shard_map/secd,efd->secf/dot_general | solution.py:207
  221.3 93.1 %all-gather.6.cloned.1.call-done = bf16[4,1024,2048]{2,1,0:T(8,128)(2,1)} async-done(((bf16[4,128,2048]{2,1,0:T(8,128)(2,1)}), bf16[4,1024,2048]{2,1,0:T(8,128)(2,1)}) %all-gather.6.cloned.1.call-update) | async-done | bytes 16777232 | tf_op jit(solution)/shard_map/all_gather | solution.py:203
  314.3 13.1 %fusion.36 = bf16[4,4,32,1024]{3,2,0,1:T(8,128)(2,1)} fusion(f32[4,4,32,1024]{3,2,1,0:T(8,128)} %fusion.26, bf16[4,1024,2048]{2,1,0:T(8,128)(2,1)} %all-gather.6.cloned.1.call-done, bf16[4,4,32,2048]{3,2,1,0:T(8,128)(2,1)S(1)} %all-to-all-done), kind=kOutput, calls=%fused_computation.42 | convolution fusion | flops 2150629376 | bytes 22020096 | tf_op jit(solution)/shard_map/secd,efd->secf/dot_general | solution.py:206
  327.4 137.8 %all-gather.10.cloned.1.call-done = bf16[4,1024,2048]{2,1,0:T(8,128)(2,1)} async-done(((bf16[4,128,2048]{2,1,0:T(8,128)(2,1)}), bf16[4,1024,2048]{2,1,0:T(8,128)(2,1)}) %all-gather.10.cloned.1.call-update) | async-done | bytes 16777232 | tf_op jit(solution)/shard_map/all_gather | solution.py:205
  465.3 8.5 %fusion.33 = bf16[4,4,32,2048]{3,2,0,1:T(8,128)(2,1)S(1)} fusion(bf16[4,4,32,1024]{3,2,0,1:T(8,128)(2,1)} %fusion.36, bf16[4,1024,2048]{2,1,0:T(8,128)(2,1)} %all-gather.10.cloned.1.call-done), kind=kOutput, calls=%fused_computation.40 | convolution fusion | flops 2148532224 | bytes 19922944 | tf_op jit(solution)/shard_map/secf,efd->secd/dot_general | solution.py:209
  473.7 1.6 copy.119
  475.3 4.0 all-to-all-start.1
  479.9 24.7 %all-to-all-done.1 = bf16[4,4,32,2048]{3,2,1,0:T(8,128)(2,1)S(1)} async-done(((bf16[4,4,32,2048]{3,2,1,0:T(8,128)(2,1)}), bf16[4,4,32,2048]{3,2,1,0:T(8,128)(2,1)S(1)}, u32[]{:S(2)}, u32[]{:S(2)}) %all-to-all-start.1) | async-done | bytes 2097184 | tf_op jit(solution)/shard_map/all_to_all | solution.py:210
  504.6 2.3 gather_fusion.1
  507.0 1.7 gather.15
  508.7 4.9 multiply_reduce_fusion
  (148 shorter events, 39.8 us)
Async XLA Ops:
  7.2 199.1 %copy-start = (bf16[256,2048]{1,0:T(8,128)(2,1)S(1)}, bf16[256,2048]{1,0:T(8,128)(2,1)}, u32[]{:S(2)}) copy-start(bf16[256,2048]{1,0:T(8,128)(2,1)} %param.27) | copy-start | bytes 3145732
  7.2 201.2 %all-gather.8.cloned.1.call-start = ((), (), s32[]{:S(2)}) async-start(), calls=%async_computation.5 | async-start | bytes 18874368 | tf_op jit(solution)/shard_map/all_gather | solution.py:204
  7.9 1.5 copy-start.11
  7.9 5.2 %copy-start.2 = (bf16[128,2048]{1,0:T(8,128)(2,1)S(1)}, bf16[128,2048]{1,0:T(8,128)(2,1)}, u32[]{:S(2)}) copy-start(bf16[128,2048]{1,0:T(8,128)(2,1)} %param.28) | copy-start | bytes 1572868
  7.9 5.4 %copy-start.14 = (f32[2048]{0:T(1024)S(1)}, f32[2048]{0:T(1024)}, u32[]{:S(2)}) copy-start(f32[2048]{0:T(1024)} %param.29) | copy-start | bytes 24580
  7.9 306.4 %all-gather.6.cloned.1.call-start = ((), (), s32[]{:S(2)}) async-start(), calls=%async_computation.4 | async-start | bytes 18874368 | tf_op jit(solution)/shard_map/all_gather | solution.py:203
  8.7 456.6 %all-gather.10.cloned.1.call-start = ((), (), s32[]{:S(2)}) async-start(), calls=%async_computation.6 | async-start | bytes 18874368 | tf_op jit(solution)/shard_map/all_gather | solution.py:205
  11.0 0.6 copy-start.9
  11.6 1.5 copy-start.17
  20.0 5.6 %copy-start.23 = (f32[2]{0:T(128)S(1)}, f32[2]{0:T(128)}, u32[]{:S(2)}) copy-start(f32[2]{0:T(128)} %param.25) | copy-start | bytes 28
  20.0 5.6 %copy-start.19 = (f32[2,512]{1,0:T(2,128)S(1)}, f32[2,512]{1,0:T(2,128)}, u32[]{:S(2)}) copy-start(f32[2,512]{1,0:T(2,128)} %param.26) | copy-start | bytes 12292
  20.0 5.6 %copy-start.20 = (bf16[2,512]{1,0:T(2,128)(2,1)S(1)}, bf16[2,512]{1,0:T(2,128)(2,1)}, u32[]{:S(2)}) copy-start(bf16[2,512]{1,0:T(2,128)(2,1)} %param.24) | copy-start | bytes 6148
  20.0 5.8 %copy-start.6 = (bf16[512,256]{1,0:T(8,128)(2,1)S(1)}, bf16[512,256]{1,0:T(8,128)(2,1)}, u32[]{:S(2)}) copy-start(bf16[512,256]{1,0:T(8,128)(2,1)} %param.21) | copy-start | bytes 786436
  20.0 188.4 %all-to-all-start = ((bf16[4,4,32,2048]{3,2,1,0:T(8,128)(2,1)}), bf16[4,4,32,2048]{3,2,1,0:T(8,128)(2,1)S(1)}, u32[]{:S(2)}, u32[]{:S(2)}) async-start(bf16[4,4,32,2048]{3,2,1,0:T(8,128)(2,1)} %broadcast_select_fusion), calls=%async_computation.1 | async-start | bytes 4194304 | tf_op jit(solution)/shard_map/all_to_all | solution.py:202
  25.6 488.0 %reduce-scatter.2.cloned.1.call-start = ((), (), s32[]{:S(2)}) async-start(), calls=%async_computation.3 | async-start | bytes 2359296 | tf_op jit(solution)/shard_map/reduce_scatter | solution.py:178
  28.6 0.6 copy-start.15
  28.7 0.8 copy-start.4
  116.8 0.6 copy-start.13
  118.1 4.3 copy-start.7
  122.4 2.0 copy-start.3
  122.4 3.1 copy-start.5
  122.4 3.1 copy-start.8
  122.4 3.1 copy-start.16
  123.6 4.0 copy-start.21
  475.3 4.0 copy-start.10
  475.3 4.2 copy-start.12
  475.3 4.4 copy-start.24
  475.3 4.4 copy-start.22
  475.3 4.6 copy-start.18
  475.3 29.3 %all-to-all-start.1 = ((bf16[4,4,32,2048]{3,2,1,0:T(8,128)(2,1)}), bf16[4,4,32,2048]{3,2,1,0:T(8,128)(2,1)S(1)}, u32[]{:S(2)}, u32[]{:S(2)}) async-start(bf16[4,4,32,2048]{3,2,1,0:T(8,128)(2,1)} %copy.119), calls=%async_computation.2 | async-start | bytes 4194304 | tf_op jit(solution)/shard_map/all_to_all | solution.py:210
  504.6 9.0 %copy-start.1 = (bf16[256,2048]{1,0:T(8,128)(2,1)S(1)}, bf16[256,2048]{1,0:T(8,128)(2,1)}, u32[]{:S(2)}) copy-start(bf16[256,2048]{1,0:T(8,128)(2,1)} %param.27) | copy-start | bytes 3145732
Sparse Core Ops, SparseCore 0:
  9.6 153.7 all-gather.7
  165.0 149.2 all-gather.5
  316.0 149.2 all-gather.9
  468.0 34.1 reduce-scatter.1
where the time goes:
time: 522 us; the launch traced here: 520 us
  waiting for transfers between devices  258 us (49%)
  other arithmetic  98.3 us (19%)
  matrix products  91.2 us (17%)
  local copies, waits for them, and re-layouts  26 us (5%)
  blocking collectives  22.5 us (4%)
  between operations  14.2 us (3%)
  starting transfers between devices  9.7 us (2%)
    all_gather x1, waiting for transfers between devices, shards(): down_piece = lax.all_gather(expert_down_weight, 'tp', axis=1, tiled=True)  138 us
    all_gather x1, waiting for transfers between devices, shards(): gate_piece = lax.all_gather(expert_gate_weight, 'tp', axis=1, tiled=True)  93.1 us
    another operation x2, other arithmetic, block_terms(): jax.scipy.linalg.solve_triangular(system, rhs_cols, lower=True, unit_diag...  80 us
    all_to_all x1, waiting for transfers between devices, shards(): lax.all_to_all(produced.astype(jnp.bfloat16), 'ep', split_axis=0, concat_...  24.7 us
    all_gather x2, blocking collectives, prefix(): pieces = jax.tree.map(lambda part: lax.all_gather(part, axis), value)  22.5 us
    dot_general x8, matrix products, carry_step(): jnp.einsum('hcj,hjv->hcv', scores, value_updates, precision=precise_setting)  14.2 us
    dot_general x1, matrix products, shards(): jnp.einsum('secd,efd->secf', arrived, gate_piece, preferred_element_type=...  13.1 us
    dot_general x1, matrix products, shards(): jnp.einsum('secd,efd->secf', arrived, up_piece, preferred_element_type=jn...  12.9 us
  transfers between devices with their start and end apart: 6, of which 3 were waited for; matrix products, arithmetic and copies ran while one was open for 41% of the time, Pallas kernels for 0%

commit v1 on v0

--- a/solution.py
+++ b/solution.py
@@ -2,6 +2,7 @@
 import jax.numpy as jnp
 from jax import lax
 from jax.sharding import PartitionSpec as P
+from jax.lax import axis_index, axis_size, ppermute
 
 DK = 128
 DV = 128
@@ -11,6 +12,18 @@
 TOPK = 2
 precise_setting = lax.Precision.HIGHEST
 norm_eps = 1e-06
+
+
+def handle_masks_all(field, body):
+    f_now, field_out = (axis_size("tp"), axis_index("tp"))
+    rack = [(ix, (ix - 1) % f_now) for ix in range(f_now)]
+    block_next = field.shape[1]
+    newest = field
+    a_next = body(newest, field_out * block_next)
+    for dev_i in range(1, f_now):
+        newest = ppermute(newest, "tp", rack)
+        a_next = a_next + body(newest, (field_out + dev_i) % f_now * block_next)
+    return a_next
 
 
 def prefix(value, axis, join, neutral):
@@ -202,11 +215,18 @@
     arrived = lax.all_to_all(outgoing, "ep", split_axis=0, concat_axis=0, tiled=True)
     gate_piece = lax.all_gather(expert_gate_weight, "tp", axis=1, tiled=True)
     up_piece = lax.all_gather(expert_up_weight, "tp", axis=1, tiled=True)
-    down_piece = lax.all_gather(expert_down_weight, "tp", axis=1, tiled=True)
     gating = jnp.einsum("secd,efd->secf", arrived, gate_piece, preferred_element_type=jnp.float32)
     upward = jnp.einsum("secd,efd->secf", arrived, up_piece, preferred_element_type=jnp.float32)
     hidden = (jax.nn.silu(gating) * upward).astype(jnp.bfloat16)
-    produced = jnp.einsum("secf,efd->secd", hidden, down_piece, preferred_element_type=jnp.float32)
+    produced = handle_masks_all(
+        expert_down_weight,
+        lambda shard, offset: jnp.einsum(
+            "secf,efd->secd",
+            lax.dynamic_slice_in_dim(hidden, offset, shard.shape[1], axis=3),
+            shard,
+            preferred_element_type=jnp.float32,
+        ),
+    )
     returned = lax.all_to_all(
         produced.astype(jnp.bfloat16), "ep", split_axis=0, concat_axis=0, tiled=True
     )

time: 522 us -> 542 us (1.038)
  the two profiles are of different devices: /device:TPU:0 before, /device:TPU:24 now
where the time goes in v1:
time: 542 us; the launch traced here: 540 us
  waiting for transfers between devices  250 us (46%)
  matrix products  112 us (21%)
  other arithmetic  100 us (18%)
  starting transfers between devices  22.3 us (4%)
  blocking collectives  22 us (4%)
  local copies, waits for them, and re-layouts  18.5 us (3%)
  between operations  14.3 us (3%)
    ppermute x7, waiting for transfers between devices, handle_masks_all(): newest = ppermute(newest, 'tp', rack)  197 us
    another operation x2, other arithmetic, block_terms(): jax.scipy.linalg.solve_triangular(system, rhs_cols, lower=True, unit_diag...  80 us
    dot_general x8, matrix products, shards(): jnp.einsum('secf,efd->secd', lax.dynamic_slice_in_dim(hidden, offset, sha...  31.6 us
    all_gather x1, waiting for transfers between devices, shards(): gate_piece = lax.all_gather(expert_gate_weight, 'tp', axis=1, tiled=True)  26.9 us
    all_to_all x1, waiting for transfers between devices, shards(): lax.all_to_all(produced.astype(jnp.bfloat16), 'ep', split_axis=0, concat_...  25 us
    all_gather x2, blocking collectives, prefix(): pieces = jax.tree.map(lambda part: lax.all_gather(part, axis), value)  22 us
    ppermute x7, starting transfers between devices, handle_masks_all(): newest = ppermute(newest, 'tp', rack)  14.5 us
    dot_general x8, matrix products, carry_step(): jnp.einsum('hcj,hjv->hcv', scores, value_updates, precision=precise_setting)  14.1 us
  transfers between devices with their start and end apart: 12, of which 6 were waited for; matrix products, arithmetic and copies ran while one was open for 43% of the time, Pallas kernels for 0%

profile of v1, /device:TPU:24, one launch (start us, length us, event | category | flops | bytes accessed | tf_op | source)
XLA Modules:
  0.0 539.6 jit_solution(5116004035360359934)
XLA Ops:
  8.9 46.6 %collective-permute-done = bf16[4,128,2048]{2,1,0:T(8,128)(2,1)} collective-permute-done((bf16[4,128,2048]{2,1,0:T(8,128)(2,1)S(1)}, bf16[4,128,2048]{2,1,0:T(8,128)(2,1)}, u32[]{:S(2)}, u32[]{:S(2)}) %collective-permute-start) | collective-permute-done | bytes 2097184 | tf_op jit(solution)/shard_map/ppermute | solution.py:24
  55.5 2.3 collective-permute-start.1
  60.8 65.9 %collective-permute-done.1 = bf16[4,128,2048]{2,1,0:T(8,128)(2,1)} collective-permute-done((bf16[4,128,2048]{2,1,0:T(8,128)(2,1)}, bf16[4,128,2048]{2,1,0:T(8,128)(2,1)}, u32[]{:S(2)}, u32[]{:S(2)}) %collective-permute-start.1) | collective-permute-done | bytes 2097184 | tf_op jit(solution)/shard_map/ppermute | solution.py:24
  126.7 2.2 collective-permute-start.2
  131.5 3.3 gather_fusion
  134.8 3.1 broadcast_select_fusion
  138.0 4.0 all-to-all-start
  142.3 55.6 %collective-permute-done.2 = bf16[4,128,2048]{2,1,0:T(8,128)(2,1)} collective-permute-done((bf16[4,128,2048]{2,1,0:T(8,128)(2,1)}, bf16[4,128,2048]{2,1,0:T(8,128)(2,1)}, u32[]{:S(2)}, u32[]{:S(2)}) %collective-permute-start.2) | collective-permute-done | bytes 2097184 | tf_op jit(solution)/shard_map/ppermute | solution.py:24
  197.9 2.2 collective-permute-start.3
  203.2 2.2 fusion.60
  206.3 28.4 %collective-permute-done.3 = bf16[4,128,2048]{2,1,0:T(8,128)(2,1)} collective-permute-done((bf16[4,128,2048]{2,1,0:T(8,128)(2,1)}, bf16[4,128,2048]{2,1,0:T(8,128)(2,1)}, u32[]{:S(2)}, u32[]{:S(2)}) %collective-permute-start.3) | collective-permute-done | bytes 2097184 | tf_op jit(solution)/shard_map/ppermute | solution.py:24
  234.8 1.9 collective-permute-start.4
  236.7 80.0 %custom-call.4 = f32[2,8,1,64,64]{3,4,2,1,0:T(8,128)} custom-call(f32[2,8,1,64,64]{4,3,2,1,0:T(8,128)} %fusion.60), custom_call_target="InvertDiagBlocksLowerTriangular" | custom-call | tf_op jit(solution)/shard_map/jit(_solve_triangular)/vmap(vmap())/triangular_solve | solution.py:65
  316.7 2.0 copy.100
  320.1 2.5 multiply_multiply_fusion
  325.7 2.0 fusion.58
  328.8 5.6 %collective-permute-start.5 = (bf16[4,128,2048]{2,1,0:T(8,128)(2,1)}, bf16[4,128,2048]{2,1,0:T(8,128)(2,1)}, u32[]{:S(2)}, u32[]{:S(2)}) collective-permute-start(bf16[4,128,2048]{2,1,0:T(8,128)(2,1)} %collective-permute-done.4), channel_id=1, source_target_pairs={{0,7},{1,0},{2,1},{3,2},{4,3},{5,4},{6,5},{7,6},{8,15},{9,8},{10,9... | collective-permute-start | bytes 6291464 | tf_op jit(solution)/shard_map/ppermute | solution.py:24
  334.4 43.4 %while.26 = (s32[]{:T(128)}, f32[2,128,256]{2,1,0:T(8,128)S(1)}, f32[8,2,64,256]{3,2,0,1:T(8,128)}, f32[8,2]{1,0:T(8,128)S(1)}, f32[8,2,64,128]{3,2,0,1:T(8,128)...) while((s32[]{:T(128)}, f32[2,128,256]{2,1,0:T(8,128)S(1)}, ...), condition=%wide.region_4.5_spmd, body=%wide.region_3.4_spmd.sunk | while | flops 176357376 | bytes 2231425 | solution.py:175
  336.9 1.8 fusion.150
  342.3 1.8 fusion.150
  347.7 1.8 fusion.150
  353.1 1.8 fusion.150
  358.5 1.8 fusion.150
  363.9 1.8 fusion.150
  369.4 1.8 fusion.150
  374.8 1.8 fusion.150
  377.9 11.5 %all-gather = f32[8,128,128]{2,1,0:T(8,128)} all-gather(f32[2,128,128]{2,1,0:T(8,128)S(1)} %get-tuple-element.243), channel_id=2, replica_groups=mesh['ep'=4,'tp'=8] {'ep'}, dimensions={0}, use_global_device_ids=true | all-gather | bytes 655360 | tf_op jit(solution)/shard_map/all_gather | solution.py:31
  389.4 10.5 %all-gather.1 = f32[8,128,128]{2,1,0:T(8,128)} all-gather(f32[2,128,128]{2,1,0:T(8,128)S(1)} %get-tuple-element.242), channel_id=3, replica_groups=mesh['ep'=4,'tp'=8] {'ep'}, dimensions={0}, use_global_device_ids=true | all-gather | bytes 655360 | tf_op jit(solution)/shard_map/all_gather | solution.py:31
  399.9 3.8 while.27
  403.7 1.8 fusion.63
  405.8 2.0 convolution_convert_fusion
  408.2 12.7 %fusion.24 = f32[4,4,32,1024]{3,2,1,0:T(8,128)} fusion(bf16[4,1024,2048]{2,1,0:T(8,128)(2,1)} %all-gather.7.cloned.1.call-done, bf16[4,4,32,2048]{3,2,1,0:T(8,128)(2,1)S(1)} %all-to-all-done), kind=kOutput, calls=%fused_computation.32 | convolution fusion | flops 2147483648 | bytes 20971520 | tf_op jit(solution)/shard_map/secd,efd->secf/dot_general | solution.py:219
  421.0 26.9 %all-gather.5.cloned.1.call-done = bf16[4,1024,2048]{2,1,0:T(8,128)(2,1)} async-done(((bf16[4,128,2048]{2,1,0:T(8,128)(2,1)}), bf16[4,1024,2048]{2,1,0:T(8,128)(2,1)}) %all-gather.5.cloned.1.call-update) | async-done | bytes 16777232 | tf_op jit(solution)/shard_map/all_gather | solution.py:216
  447.9 12.1 %fusion.44 = bf16[4,4,32,1024]{3,2,0,1:T(8,128)(2,1)S(1)} fusion(f32[4,4,32,1024]{3,2,1,0:T(8,128)} %fusion.24, bf16[4,1024,2048]{2,1,0:T(8,128)(2,1)} %all-gather.5.cloned.1.call-done, bf16[4,4,32,2048]{3,2,1,0:T(8,128)(2,1)S(1)} %all-to-all-done), kind=kOutput, calls=%fused_computation.55 | convolution fusion | flops 2150629376 | bytes 22020096 | tf_op jit(solution)/shard_map/secd,efd->secf/dot_general | solution.py:218
  460.0 2.3 fusion.42
  462.3 2.3 fusion.30
  464.7 2.3 fusion.32
  467.0 2.3 fusion.34
  469.3 4.3 fusion.36
  473.6 4.3 fusion.38
  477.8 4.5 fusion.40
  482.4 9.2 %fusion.28 = bf16[4,4,32,2048]{3,2,0,1:T(8,128)(2,1)} fusion(f32[4,4,32,2048]{3,2,1,0:T(8,128)S(1)} %fusion.30, f32[4,4,32,2048]{3,2,1,0:T(8,128)S(1)} %fusion.32, f32[4,4,32,2048]{3,2,1,0:T(8,128)S(1)} %fusion.34, f32[4,4,32,2048]{3,2,1,0:T(8,128)} %fusion.36, f32[4,4,32,2048]{3,2,1,0:T(8,128)} %fusion.38, f32[4,4,32,2048]{3,2,1,0:T(8,128)S(1)} %fusion.42, ...), kind=kOutput, calls=%fused_computation.38 | convolution fusion | flops 276824064 | bytes 33685508 | tf_op jit(solution)/shard_map/secf,efd->secd/dot_general | solution.py:223
  491.6 3.2 copy.119
  494.8 3.7 all-to-all-start.1
  499.0 25.0 %all-to-all-done.1 = bf16[4,4,32,2048]{3,2,1,0:T(8,128)(2,1)S(1)} async-done(((bf16[4,4,32,2048]{3,2,1,0:T(8,128)(2,1)}), bf16[4,4,32,2048]{3,2,1,0:T(8,128)(2,1)S(1)}, u32[]{:S(2)}, u32[]{:S(2)}) %all-to-all-start.1) | async-done | bytes 2097184 | tf_op jit(solution)/shard_map/all_to_all | solution.py:230
  524.0 2.3 gather_fusion.1
  526.4 1.7 gather.15
  528.1 4.9 multiply_reduce_fusion
  (150 shorter events, 50.9 us)
Async XLA Ops:
  7.2 398.6 %copy-start = (bf16[256,2048]{1,0:T(8,128)(2,1)S(1)}, bf16[256,2048]{1,0:T(8,128)(2,1)}, u32[]{:S(2)}) copy-start(bf16[256,2048]{1,0:T(8,128)(2,1)} %param.27) | copy-start | bytes 3145732
  7.2 1.7 copy-start.2
  7.2 50.6 %copy-start.8 = (s32[128,2]{0,1:T(2,128)S(1)}, s32[128,2]{0,1:T(2,128)}, u32[]{:S(2)}) copy-start(s32[128,2]{0,1:T(2,128)} %param.30) | copy-start | bytes 3076
  7.2 123.1 %copy-start.9 = (f32[2048]{0:T(1024)S(1)}, f32[2048]{0:T(1024)}, u32[]{:S(2)}) copy-start(f32[2048]{0:T(1024)} %param.29) | copy-start | bytes 24580
  7.2 401.0 %all-gather.7.cloned.1.call-start = ((), (), s32[]{:S(2)}) async-start(), calls=%async_computation.5 | async-start | bytes 18874368 | tf_op jit(solution)/shard_map/all_gather | solution.py:217
  7.9 440.0 %all-gather.5.cloned.1.call-start = ((), (), s32[]{:S(2)}) async-start(), calls=%async_computation.4 | async-start | bytes 18874368 | tf_op jit(solution)/shard_map/all_gather | solution.py:216
  8.9 46.6 %collective-permute-start = (bf16[4,128,2048]{2,1,0:T(8,128)(2,1)S(1)}, bf16[4,128,2048]{2,1,0:T(8,128)(2,1)}, u32[]{:S(2)}, u32[]{:S(2)}) collective-permute-start(bf16[4,128,2048]{2,1,0:T(8,128)(2,1)S(1)} %copy-done.2), channel_id=1, source_target_pairs={{0,7},{1,0},{2,1},{3,2},{4,3},{5,4},{6,5},{7,6},{8,15},{9,8},{10,9... | collective-permute-start | bytes 6291464 | tf_op jit(solution)/shard_map/ppermute | solution.py:24
  55.5 71.2 %collective-permute-start.1 = (bf16[4,128,2048]{2,1,0:T(8,128)(2,1)}, bf16[4,128,2048]{2,1,0:T(8,128)(2,1)}, u32[]{:S(2)}, u32[]{:S(2)}) collective-permute-start(bf16[4,128,2048]{2,1,0:T(8,128)(2,1)} %collective-permute-done), channel_id=1, source_target_pairs={{0,7},{1,0},{2,1},{3,2},{4,3},{5,4},{6,5},{7,6},{8,15},{9,8},{10,9... | collective-permute-start | bytes 6291464 | tf_op jit(solution)/shard_map/ppermute | solution.py:24
  126.7 71.1 %collective-permute-start.2 = (bf16[4,128,2048]{2,1,0:T(8,128)(2,1)}, bf16[4,128,2048]{2,1,0:T(8,128)(2,1)}, u32[]{:S(2)}, u32[]{:S(2)}) collective-permute-start(bf16[4,128,2048]{2,1,0:T(8,128)(2,1)} %collective-permute-done.1), channel_id=1, source_target_pairs={{0,7},{1,0},{2,1},{3,2},{4,3},{5,4},{6,5},{7,6},{8,15},{9,8},{10,9... | collective-permute-start | bytes 6291464 | tf_op jit(solution)/shard_map/ppermute | solution.py:24
  137.9 4.0 copy-start.6
  137.9 4.2 copy-start.15
  138.0 4.3 copy-start.10
  138.0 4.3 copy-start.12
  138.0 62.3 %copy-start.11 = (bf16[2,512]{1,0:T(2,128)(2,1)S(1)}, bf16[2,512]{1,0:T(2,128)(2,1)}, u32[]{:S(2)}) copy-start(bf16[2,512]{1,0:T(2,128)(2,1)} %param.23) | copy-start | bytes 6148
  138.0 270.2 %all-to-all-start = ((bf16[4,4,32,2048]{3,2,1,0:T(8,128)(2,1)}), bf16[4,4,32,2048]{3,2,1,0:T(8,128)(2,1)S(1)}, u32[]{:S(2)}, u32[]{:S(2)}) async-start(bf16[4,4,32,2048]{3,2,1,0:T(8,128)(2,1)} %broadcast_select_fusion), calls=%async_computation.1 | async-start | bytes 4194304 | tf_op jit(solution)/shard_map/all_to_all | solution.py:215
  142.0 391.0 %reduce-scatter.2.cloned.1.call-start = ((), (), s32[]{:S(2)}) async-start(), calls=%async_computation.3 | async-start | bytes 2359296 | tf_op jit(solution)/shard_map/reduce_scatter | solution.py:191
  197.9 36.9 %collective-permute-start.3 = (bf16[4,128,2048]{2,1,0:T(8,128)(2,1)}, bf16[4,128,2048]{2,1,0:T(8,128)(2,1)}, u32[]{:S(2)}, u32[]{:S(2)}) collective-permute-start(bf16[4,128,2048]{2,1,0:T(8,128)(2,1)} %collective-permute-done.2), channel_id=1, source_target_pairs={{0,7},{1,0},{2,1},{3,2},{4,3},{5,4},{6,5},{7,6},{8,15},{9,8},{10,9... | collective-permute-start | bytes 6291464 | tf_op jit(solution)/shard_map/ppermute | solution.py:24
  203.2 3.1 copy-start.4
  234.8 94.0 %collective-permute-start.4 = (bf16[4,128,2048]{2,1,0:T(8,128)(2,1)}, bf16[4,128,2048]{2,1,0:T(8,128)(2,1)}, u32[]{:S(2)}, u32[]{:S(2)}) collective-permute-start(bf16[4,128,2048]{2,1,0:T(8,128)(2,1)} %collective-permute-done.3), channel_id=1, source_target_pairs={{0,7},{1,0},{2,1},{3,2},{4,3},{5,4},{6,5},{7,6},{8,15},{9,8},{10,9... | collective-permute-start | bytes 6291464 | tf_op jit(solution)/shard_map/ppermute | solution.py:24
  318.9 3.6 copy-start.7
  322.5 2.0 copy-start.3
  322.5 3.2 copy-start.5
  323.6 4.0 copy-start.13
  328.8 79.2 %collective-permute-start.5 = (bf16[4,128,2048]{2,1,0:T(8,128)(2,1)}, bf16[4,128,2048]{2,1,0:T(8,128)(2,1)}, u32[]{:S(2)}, u32[]{:S(2)}) collective-permute-start(bf16[4,128,2048]{2,1,0:T(8,128)(2,1)} %collective-permute-done.4), channel_id=1, source_target_pairs={{0,7},{1,0},{2,1},{3,2},{4,3},{5,4},{6,5},{7,6},{8,15},{9,8},{10,9... | collective-permute-start | bytes 6291464 | tf_op jit(solution)/shard_map/ppermute | solution.py:24
  408.0 74.4 %collective-permute-start.6 = (bf16[4,128,2048]{2,1,0:T(8,128)(2,1)}, bf16[4,128,2048]{2,1,0:T(8,128)(2,1)}, u32[]{:S(2)}, u32[]{:S(2)}) collective-permute-start(bf16[4,128,2048]{2,1,0:T(8,128)(2,1)} %collective-permute-done.5), channel_id=1, source_target_pairs={{0,7},{1,0},{2,1},{3,2},{4,3},{5,4},{6,5},{7,6},{8,15},{9,8},{10,9... | collective-permute-start | bytes 6291464 | tf_op jit(solution)/shard_map/ppermute | solution.py:24
  494.8 4.1 copy-start.16
  494.8 4.1 copy-start.14
  494.8 29.3 %all-to-all-start.1 = ((bf16[4,4,32,2048]{3,2,1,0:T(8,128)(2,1)}), bf16[4,4,32,2048]{3,2,1,0:T(8,128)(2,1)S(1)}, u32[]{:S(2)}, u32[]{:S(2)}) async-start(bf16[4,4,32,2048]{3,2,1,0:T(8,128)(2,1)} %copy.119), calls=%async_computation.2 | async-start | bytes 4194304 | tf_op jit(solution)/shard_map/all_to_all | solution.py:230
  524.0 9.0 %copy-start.1 = (bf16[256,2048]{1,0:T(8,128)(2,1)S(1)}, bf16[256,2048]{1,0:T(8,128)(2,1)}, u32[]{:S(2)}) copy-start(bf16[256,2048]{1,0:T(8,128)(2,1)} %param.27) | copy-start | bytes 3145732
Sparse Core Ops, SparseCore 0:
  9.6 231.0 all-gather.6
  242.3 205.5 all-gather.4
  450.8 31.3 reduce-scatter.1
